TPU v7x, 32 devices: a whole 2x2x4 slice. The times are simulated.
32 devices in a mesh: fs: 16 (over z, y, x), tp: 2 (over core).
Axes of the slice: x: 2, y: 2, z: 4, core: 2. Of those that a mesh axis runs over, the one named last changes fastest.
Arguments:
- tokens: bfloat16 [2, 256, 2048], P('tp'), may hold values from -6 to 6
- gain_first: float32 [2048], P('fs'), may hold values from 0.1 to 1.9
- gate_first: float32 [2048, 5632], P('fs', 'tp'), may hold values from -0.125 to 0.125
- up_first: float32 [2048, 5632], P('fs', 'tp'), may hold values from -0.125 to 0.125
- down_first: float32 [2048, 5632], P('fs', 'tp'), may hold values from -0.3125 to 0.3125
- gain_second: float32 [2048], P('fs'), may hold values from 0.1 to 1.9
- gate_second: float32 [2048, 5632], P('fs', 'tp'), may hold values from -0.125 to 0.125
- up_second: float32 [2048, 5632], P('fs', 'tp'), may hold values from -0.125 to 0.125
- down_second: float32 [2048, 5632], P('fs', 'tp'), may hold values from -0.3125 to 0.3125
Outputs:
- mixed: bfloat16 [2, 256, 2048], P('tp', 'fs')
- served_gate_first: bfloat16 [2, 2816, 2048], P(None, 'fs')
- served_up_first: bfloat16 [2, 2816, 2048], P(None, 'fs')
- served_down_first: bfloat16 [2, 2816, 2048], P(None, 'fs')
- served_gate_second: bfloat16 [2, 2816, 2048], P(None, 'fs')
- served_up_second: bfloat16 [2, 2816, 2048], P(None, 'fs')
- served_down_second: bfloat16 [2, 2816, 2048], P(None, 'fs')
All inputs are finite; a program needn't handle non-finite values.
Results may differ from a plain program's by a relative error of at most 0.013.
Values may be sent and summed in bfloat16 or wider, within the bound.
A program may use at most 64 MiB of HBM per device.

v0:
```python
import functools
import math

import jax
import jax.numpy as jnp
from jax import lax
from jax.experimental import pallas as pl
from jax.experimental.pallas import tpu as pltpu
from jax.sharding import PartitionSpec as P


def normalize(values):
    wide = values.astype(jnp.float32)
    scale = lax.rsqrt(jnp.mean(wide * wide, axis=-1, keepdims=True) + 1e-06)
    return (wide * scale).astype(jnp.bfloat16)


def folded(weight, gain):
    return (weight * gain[:, None]).astype(jnp.bfloat16).T


def relayout(gate_part, up_part, down_part):
    gate_cut, up_cut, down_cut = (
        lax.all_to_all(gate_part, "fs", split_axis=0, concat_axis=1, tiled=True),
        lax.all_to_all(up_part, "fs", split_axis=0, concat_axis=1, tiled=True),
        lax.all_to_all(down_part, "fs", split_axis=0, concat_axis=1, tiled=True),
    )
    return (
        lax.all_gather(gate_cut[None], "tp", axis=0, tiled=True),
        lax.all_gather(up_cut[None], "tp", axis=0, tiled=True),
        lax.all_gather(down_cut[None], "tp", axis=0, tiled=True),
    )


def hidden_of(normed, gate_served, up_served):
    gate_flat = gate_served.reshape(-1, gate_served.shape[2])
    up_flat = up_served.reshape(-1, up_served.shape[2])
    gate_act = jnp.einsum("rd,hd->rh", normed, gate_flat, preferred_element_type=jnp.float32)
    up_act = jnp.einsum("rd,hd->rh", normed, up_flat, preferred_element_type=jnp.float32)
    return (jax.nn.silu(gate_act) * up_act).astype(jnp.bfloat16)


def projector(hidden, down_flat):
    return jnp.dot(hidden, down_flat, preferred_element_type=jnp.float32)


def shards(
    tokens,
    gain_first,
    gate_first,
    up_first,
    down_first,
    gain_second,
    gate_second,
    up_second,
    down_second,
):
    gate_one, up_one, down_one = relayout(
        folded(gate_first, gain_first),
        folded(up_first, gain_first),
        down_first.astype(jnp.bfloat16).T,
    )
    gate_two, up_two, down_two = relayout(
        folded(gate_second, gain_second),
        folded(up_second, gain_second),
        down_second.astype(jnp.bfloat16).T,
    )
    rows = tokens[0]
    keep = rows.shape[0] // lax.axis_size("fs")
    offset = lax.axis_index("fs") * keep
    hidden_first = hidden_of(normalize(rows), gate_one, up_one)
    down_flat_one = down_one.reshape(-1, down_one.shape[2])
    partial_value = jnp.dot(hidden_first, down_flat_one, preferred_element_type=jnp.float32)
    branch = lax.psum(partial_value, "fs")
    whole_middle = (rows.astype(jnp.float32) + 0.5 * branch).astype(jnp.bfloat16)
    hidden_second = hidden_of(normalize(whole_middle), gate_two, up_two)
    middle = lax.dynamic_slice_in_dim(whole_middle, offset, keep, 0)
    down_flat_two = down_two.reshape(-1, down_two.shape[2])
    branch_two = lax.psum_scatter(
        projector(hidden_second, down_flat_two), "fs", scatter_dimension=0, tiled=True
    )
    mixed = (middle.astype(jnp.float32) + 0.5 * branch_two).astype(jnp.bfloat16)[None]
    return (mixed, gate_one, up_one, down_one, gate_two, up_two, down_two)


def loop(lo, hi, body):
    lax.fori_loop(lo, hi, lambda i, c: (body(i), c)[1], 0)


def step_kernel(
    n,
    inner,
    tokens_ref,
    gain_one_ref,
    gain_two_ref,
    w0,
    w1,
    w2,
    w3,
    w4,
    w5,
    mixed_ref,
    o0,
    o1,
    o2,
    o3,
    o4,
    o5,
    raw,
    cut,
    served,
    normed,
    gate_acc,
    up_acc,
    hidden,
    middle,
    part,
    plane_in,
    plane_sum,
    line_in,
    load_sem,
    store_sem,
    send_sem,
    recv_sem,
    pass_send,
    pass_recv,
    ring_send,
    ring_recv,
):
    outer = n // inner
    me = lax.axis_index("fs")
    core = lax.axis_index("tp")
    row = me // inner
    col = lax.rem(me, inner)
    weights = (w0, w1, w2, w3, w4, w5)
    outs = (o0, o1, o2, o3, o4, o5)
    rows = served.shape[2]
    feats = cut.shape[2]
    depth = normed.shape[1]
    mine = pl.ds(pl.multiple_of(me * feats, feats), feats)

    def load(a):
        return pltpu.make_async_copy(weights[a], raw.at[a], load_sem.at[a])

    def store(a):
        return pltpu.make_async_copy(served.at[a], outs[a], store_sem.at[a])

    def cast(a):
        load(a).wait()
        gain = gain_one_ref if a < 3 else gain_two_ref

        count = raw.shape[2] // 128
        per = next(d for d in (11, 4, 2, 1) if count % d == 0)
        spread = jnp.broadcast_to(gain[...], (128, feats)).T

        def tile(i):
            for piece in range(per):
                at = pl.ds(pl.multiple_of((i * per + piece) * 128, 128), 128)
                block = raw[a, :, at]
                if a % 3 != 2:
                    block = block * spread
                cut[a, at, :] = block.astype(jnp.bfloat16).T

        loop(0, count // per, tile)
        served[a, core, :, mine] = cut[a, pl.ds(pl.multiple_of(me * rows, rows), rows), :]

    def block_copy(a, j):
        k = lax.rem(j, outer) * inner + j // outer
        to = lax.rem(me + k, n)
        return pltpu.make_async_remote_copy(
            src_ref=cut.at[a, pl.ds(pl.multiple_of(to * rows, rows), rows), :],
            dst_ref=served.at[a, core, :, mine],
            send_sem=send_sem.at[a, j],
            recv_sem=recv_sem.at[a, j],
            device_id={"fs": to},
            device_id_type=pl.DeviceIdType.MESH,
        )

    def send(a):
        loop(1, n, lambda j: block_copy(a, j).start())

    def pass_copy(a):
        return pltpu.make_async_remote_copy(
            src_ref=served.at[a, core],
            dst_ref=served.at[a, core],
            send_sem=pass_send.at[a],
            recv_sem=pass_recv.at[a],
            device_id={"tp": 1 - core},
            device_id_type=pl.DeviceIdType.MESH,
        )

    def arrive(a):
        loop(1, n, lambda j: block_copy(a, j).wait_recv())
        pass_copy(a).start()

    def complete(a):
        pass_copy(a).wait_recv()
        store(a).start()

    def ring_copy(stage, k, src, dst, to):
        return pltpu.make_async_remote_copy(
            src_ref=src,
            dst_ref=dst,
            send_sem=ring_send.at[stage, k],
            recv_sem=ring_recv.at[stage, k],
            device_id={"fs": to},
            device_id_type=pl.DeviceIdType.MESH,
        )

    def plane_copies(half):
        copies = []
        for k in range(1, inner):
            to = lax.rem(col + k, inner)
            copies.append(
                ring_copy(half, k, part.at[half, to], plane_in.at[half, k - 1], row * inner + to)
            )
        return copies

    def line_copies(half):
        copies = []
        for k in range(1, outer):
            to = lax.rem(row + k, outer)
            copies.append(
                ring_copy(
                    2 + half, k, plane_sum.at[half, to], line_in.at[half, k - 1], to * inner + col
                )
            )
        return copies

    def spread_line():
        spot = middle.at[col, row]
        return [
            ring_copy(4, k, spot, spot, lax.rem(row + k, outer) * inner + col)
            for k in range(1, outer)
        ]

    def spread_plane():
        spot = middle.at[col]
        return [
            ring_copy(5, k, spot, spot, row * inner + lax.rem(col + k, inner))
            for k in range(1, inner)
        ]

    keep = tokens_ref.shape[2]

    def normalize_rows(pick):
        def one(i):
            wide = pick(i // outer, lax.rem(i, outer)).astype(jnp.float32)
            scale = lax.rsqrt(jnp.mean(wide * wide, axis=-1, keepdims=True) + 1e-06)
            at = pl.ds(pl.multiple_of(i * keep, keep), keep)
            normed[at, :] = (wide * scale).astype(jnp.bfloat16)

        loop(0, n, one)

    def expand(g, u):
        gate_acc[...] = jnp.zeros_like(gate_acc)
        up_acc[...] = jnp.zeros_like(up_acc)
        wide = 256

        def one(i):
            at = pl.ds(pl.multiple_of(i * wide, wide), wide)
            left = normed[:, at]
            for acc, a in ((gate_acc, g), (up_acc, u)):
                right = served[a, :, :, at].reshape(-1, wide)
                acc[...] += lax.dot_general(
                    left, right, (((1,), (1,)), ((), ())), preferred_element_type=jnp.float32
                )

        loop(0, depth // wide, one)
        gate = gate_acc[...]
        hidden[...] = (gate / (1.0 + jnp.exp(-gate)) * up_acc[...]).astype(jnp.bfloat16)

    def contract(d, half):
        wide = 256

        def one(i):
            at = pl.ds(pl.multiple_of(i * wide, wide), wide)
            right = served[d, :, :, at].reshape(-1, wide)
            value = jnp.dot(hidden[...], right, preferred_element_type=jnp.float32)
            part[half, :, :, :, at] = value.astype(jnp.bfloat16).reshape(inner, outer, keep, wide)

        loop(0, depth // wide, one)

    def sum_plane(half):
        def one(i):
            total = part[half, col, i].astype(jnp.float32)
            for k in range(inner - 1):
                total += plane_in[half, k, i].astype(jnp.float32)
            plane_sum[half, i] = total.astype(jnp.bfloat16)

        loop(0, outer, one)

    def sum_line(half):
        total = plane_sum[half, row].astype(jnp.float32)
        for k in range(outer - 1):
            total += line_in[half, k].astype(jnp.float32)
        return total

    def start(copies):
        for copy in copies:
            copy.start()

    def receive(copies):
        for copy in copies:
            copy.wait_recv()

    for a in range(6):
        load(a).start()
    for a in range(4):
        cast(a)
        send(a)
    cast(4)
    cast(5)
    normalize_rows(lambda c, r: tokens_ref[r, c])
    arrive(0)
    arrive(1)
    complete(0)
    complete(1)
    expand(0, 1)
    arrive(2)
    complete(2)
    contract(2, 0)
    start(plane_copies(0))
    send(4)
    receive(plane_copies(0))
    sum_plane(0)
    start(line_copies(0))
    receive(line_copies(0))
    own = tokens_ref[row, col].astype(jnp.float32) + 0.5 * sum_line(0)
    middle[col, row] = own.astype(jnp.bfloat16)
    start(spread_line())
    receive(spread_line())
    start(spread_plane())
    send(5)
    arrive(3)
    receive(spread_plane())
    normalize_rows(lambda c, r: middle[c, r])
    arrive(4)
    complete(3)
    complete(4)
    expand(3, 4)
    arrive(5)
    complete(5)
    contract(5, 1)
    start(plane_copies(1))
    receive(plane_copies(1))
    sum_plane(1)
    start(line_copies(1))
    receive(line_copies(1))
    last = middle[col, row].astype(jnp.float32) + 0.5 * sum_line(1)
    mixed_ref[...] = last.astype(jnp.bfloat16)

    for a in range(6):
        store(a).wait()
        pass_copy(a).wait_send()
        loop(1, n, lambda j, a=a: block_copy(a, j).wait_send())
    for copies in (
        plane_copies(0),
        plane_copies(1),
        line_copies(0),
        line_copies(1),
        spread_line(),
        spread_plane(),
    ):
        for copy in copies:
            copy.wait_send()


def hand_on(*refs):
    half = len(refs) // 2
    for source, target in zip(refs[:half], refs[half:]):
        target[...] = source[...]


def fused_shards(tokens, gain_first, gate_first, up_first, down_first,
                 gain_second, gate_second, up_second, down_second):
    n = lax.axis_size("fs")
    tp = lax.axis_size("tp")
    inner = math.isqrt(n)
    outer = n // inner
    feats, units = gate_first.shape
    rows = units // n
    plen, depth = tokens.shape[1], tokens.shape[2]
    keep = plen // n
    bf16, f32 = jnp.bfloat16, jnp.float32
    shuffled = tokens[0].reshape(outer, inner, keep, depth)
    vmem = pl.BlockSpec(memory_space=pltpu.VMEM)
    anywhere = pl.BlockSpec(memory_space=pl.ANY)
    served_shape = jax.ShapeDtypeStruct((tp, rows, depth), bf16)
    hid = tp * rows
    dma = pltpu.SemaphoreType.DMA
    width = max(inner, outer)
    results = pl.pallas_call(
        functools.partial(step_kernel, n, inner),
        out_shape=(jax.ShapeDtypeStruct((keep, depth), bf16),) + (served_shape,) * 6,
        in_specs=[vmem] * 3 + [anywhere] * 6,
        out_specs=(vmem,) + (anywhere,) * 6,
        scratch_shapes=[
            pltpu.VMEM((6, feats, units), f32),
            pltpu.VMEM((6, units, feats), bf16),
            pltpu.VMEM((6, tp, rows, depth), bf16),
            pltpu.VMEM((plen, depth), bf16),
            pltpu.VMEM((plen, hid), f32),
            pltpu.VMEM((plen, hid), f32),
            pltpu.VMEM((plen, hid), bf16),
            pltpu.VMEM((inner, outer, keep, depth), bf16),
            pltpu.VMEM((2, inner, outer, keep, depth), bf16),
            pltpu.VMEM((2, inner - 1, outer, keep, depth), bf16),
            pltpu.VMEM((2, outer, keep, depth), bf16),
            pltpu.VMEM((2, outer - 1, keep, depth), bf16),
            dma((6,)),
            dma((6,)),
            dma((6, n)),
            dma((6, n)),
            dma((6,)),
            dma((6,)),
            dma((6, width)),
            dma((6, width)),
        ],
        compiler_params=pltpu.CompilerParams(
            has_side_effects=True, vmem_limit_bytes=58 * 1024 * 1024
        ),
    )(
        shuffled,
        gain_first.reshape(1, feats),
        gain_second.reshape(1, feats),
        gate_first,
        up_first,
        down_first,
        gate_second,
        up_second,
        down_second,
    )
    block = pl.BlockSpec((1, rows, depth // 2), lambda i, j: (i, 0, j))
    copies = pl.pallas_call(
        hand_on,
        grid=(tp, 2),
        out_shape=(served_shape,) * 6,
        in_specs=[block] * 6,
        out_specs=(block,) * 6,
    )(*results[1:])
    return (results[0][None],) + tuple(copies)


def fits(mesh, tokens, gate):
    n, tp = mesh.shape["fs"], mesh.shape["tp"]
    inner = math.isqrt(n)
    depth, hidden = gate.shape
    plen = tokens.shape[1]
    if tp != 2 or inner < 2 or n % inner or depth % (n * 128) or hidden % (tp * n * 16):
        return False
    if depth % 256 or (hidden // tp) % 128 or plen % (n * 16) or tokens.shape[0] != tp:
        return False
    local = depth // n * (hidden // tp)
    need = local * 6 * 4 + local * 6 * 2 + local * 6 * 2 * tp
    need += plen * depth * 2 * 10 + plen * (hidden // n) * 12
    return need < 40 * 1024 * 1024


def solution(mesh):
    def run(body):
        return jax.shard_map(
            body,
            mesh=mesh,
            in_specs=(
                P("tp", None, None),
                P("fs"),
                P("fs", "tp"),
                P("fs", "tp"),
                P("fs", "tp"),
                P("fs"),
                P("fs", "tp"),
                P("fs", "tp"),
                P("fs", "tp"),
            ),
            out_specs=(
                P("tp", "fs", None),
                P(None, "fs", None),
                P(None, "fs", None),
                P(None, "fs", None),
                P(None, "fs", None),
                P(None, "fs", None),
                P(None, "fs", None),
            ),
            check_vma=False,
        )

    def step(*args):
        return run(fused_shards if fits(mesh, args[0], args[2]) else shards)(*args)

    return step
```

profile of v0, /device:TPU:0, one launch (start us, length us, event | category | flops | bytes accessed | tf_op | source)
XLA Modules:
  0.0 169.3 jit_solution(1170256936210309153)
XLA Ops:
  0.6 160.9 %shard_map.144 = (bf16[16,2048]{1,0:T(8,128)(2,1)}, bf16[2,176,2048]{2,1,0:T(8,128)(2,1)}, bf16[2,176,2048]{2,1,0:T(8,128)(2,1)}, bf16[2,176,2048]{2,1,0:T(8,128...) custom-call(bf16[4,4,16,2048]{3,2,1,0:T(8,128)(2,1)} %bitcast.4, ...), custom_call_target="tpu_custom_call" | custom-call | tf_op jit(solution)/shard_map/pallas_call | solution.py:393
  161.5 0.0 copy-start
  161.5 7.1 %shard_map.145 = (bf16[2,176,2048]{2,1,0:T(8,128)(2,1)}, bf16[2,176,2048]{2,1,0:T(8,128)(2,1)}, bf16[2,176,2048]{2,1,0:T(8,128)(2,1)}, bf16[2,176,2048]{2,1,0:T(...) custom-call(bf16[2,176,2048]{2,1,0:T(8,128)(2,1)} %get-tuple-element.21.refs_0_, ...), custom_call_target="tpu_custom_call" | custom-call | tf_op jit(solution)/shard_map/pallas_call | solution.py:435
  168.6 0.0 copy-done
  168.7 0.6 copy.17
Async XLA Ops:
  161.5 7.1 %copy-start = (bf16[16,2048]{1,0:T(8,128)(2,1)S(1)}, bf16[16,2048]{1,0:T(8,128)(2,1)}, u32[]{:S(2)}) copy-start(bf16[16,2048]{1,0:T(8,128)(2,1)} %get-tuple-element.20) | copy-start | bytes 196612
where the time goes:
time: 169 us
  Pallas kernels  168 us (99%)
    pallas_call x1, Pallas kernels, fused_shards(): pl.pallas_call(functools.partial(step_kernel, n, inner), out_shape=(jax.S...  161 us
    pallas_call x1, Pallas kernels, fused_shards(): pl.pallas_call(hand_on, grid=(tp, 2), out_shape=(served_shape,) * 6, in_s...  7.1 us

commit v1 on v0

v1 whole, which is shorter than its diff:
```python
import functools
import math

import jax
import jax.numpy as jnp
from jax import lax
from jax.experimental import pallas as pl
from jax.experimental.pallas import tpu as pltpu
from jax.sharding import PartitionSpec as P


def normalize(values):
    wide = values.astype(jnp.float32)
    scale = lax.rsqrt(jnp.mean(wide * wide, axis=-1, keepdims=True) + 1e-06)
    return (wide * scale).astype(jnp.bfloat16)


def folded(weight, gain):
    return (weight * gain[:, None]).astype(jnp.bfloat16).T


def relayout(gate_part, up_part, down_part):
    gate_cut, up_cut, down_cut = (
        lax.all_to_all(gate_part, "fs", split_axis=0, concat_axis=1, tiled=True),
        lax.all_to_all(up_part, "fs", split_axis=0, concat_axis=1, tiled=True),
        lax.all_to_all(down_part, "fs", split_axis=0, concat_axis=1, tiled=True),
    )
    return (
        lax.all_gather(gate_cut[None], "tp", axis=0, tiled=True),
        lax.all_gather(up_cut[None], "tp", axis=0, tiled=True),
        lax.all_gather(down_cut[None], "tp", axis=0, tiled=True),
    )


def hidden_of(normed, gate_served, up_served):
    gate_flat = gate_served.reshape(-1, gate_served.shape[2])
    up_flat = up_served.reshape(-1, up_served.shape[2])
    gate_act = jnp.einsum("rd,hd->rh", normed, gate_flat, preferred_element_type=jnp.float32)
    up_act = jnp.einsum("rd,hd->rh", normed, up_flat, preferred_element_type=jnp.float32)
    return (jax.nn.silu(gate_act) * up_act).astype(jnp.bfloat16)


def projector(hidden, down_flat):
    return jnp.dot(hidden, down_flat, preferred_element_type=jnp.float32)


def shards(
    tokens,
    gain_first,
    gate_first,
    up_first,
    down_first,
    gain_second,
    gate_second,
    up_second,
    down_second,
):
    gate_one, up_one, down_one = relayout(
        folded(gate_first, gain_first),
        folded(up_first, gain_first),
        down_first.astype(jnp.bfloat16).T,
    )
    gate_two, up_two, down_two = relayout(
        folded(gate_second, gain_second),
        folded(up_second, gain_second),
        down_second.astype(jnp.bfloat16).T,
    )
    rows = tokens[0]
    keep = rows.shape[0] // lax.axis_size("fs")
    offset = lax.axis_index("fs") * keep
    hidden_first = hidden_of(normalize(rows), gate_one, up_one)
    down_flat_one = down_one.reshape(-1, down_one.shape[2])
    partial_value = jnp.dot(hidden_first, down_flat_one, preferred_element_type=jnp.float32)
    branch = lax.psum(partial_value, "fs")
    whole_middle = (rows.astype(jnp.float32) + 0.5 * branch).astype(jnp.bfloat16)
    hidden_second = hidden_of(normalize(whole_middle), gate_two, up_two)
    middle = lax.dynamic_slice_in_dim(whole_middle, offset, keep, 0)
    down_flat_two = down_two.reshape(-1, down_two.shape[2])
    branch_two = lax.psum_scatter(
        projector(hidden_second, down_flat_two), "fs", scatter_dimension=0, tiled=True
    )
    mixed = (middle.astype(jnp.float32) + 0.5 * branch_two).astype(jnp.bfloat16)[None]
    return (mixed, gate_one, up_one, down_one, gate_two, up_two, down_two)


def loop(lo, hi, body):
    lax.fori_loop(lo, hi, lambda i, c: (body(i), c)[1], 0)


def step_kernel(
    n,
    inner,
    early,
    mid,
    late,
    tokens_hbm,
    gain_one_hbm,
    gain_two_hbm,
    w0,
    w1,
    w2,
    w3,
    w4,
    w5,
    mixed_ref,
    o0,
    o1,
    o2,
    o3,
    o4,
    o5,
    raw,
    cut,
    tokens_ref,
    gains,
    normed,
    hidden,
    middle,
    part,
    plane_in,
    plane_sum,
    line_in,
    load_sem,
    side_sem,
    send_sem,
    recv_sem,
    pass_send,
    pass_recv,
    plane_send,
    plane_recv,
    line_send,
    line_recv,
    spread_send,
    spread_recv,
):
    outer = n // inner
    me = lax.axis_index("fs")
    core = lax.axis_index("tp")
    row = me // inner
    col = lax.rem(me, inner)
    weights = (w0, w1, w2, w3, w4, w5)
    served = (o0, o1, o2, o3, o4, o5)
    rows = o0.shape[1]
    feats = cut.shape[2]
    depth = normed.shape[1]
    keep = tokens_ref.shape[2]
    band = depth // outer
    mine = pl.ds(pl.multiple_of(me * feats, feats), feats)
    planes = (row, row + 1 - 2 * lax.rem(row, 2), outer - 1 - row, lax.rem(row + 2, outer))

    def columns(g):
        return pl.ds(pl.multiple_of(planes[g] * band, band), band)

    def load(a):
        return pltpu.make_async_copy(weights[a], raw.at[a], load_sem.at[a])

    side_loads = (
        pltpu.make_async_copy(gain_one_hbm, gains.at[0], side_sem.at[0]),
        pltpu.make_async_copy(gain_two_hbm, gains.at[1], side_sem.at[1]),
        pltpu.make_async_copy(tokens_hbm, tokens_ref, side_sem.at[2]),
    )

    def cast(a):
        load(a).wait()
        count = raw.shape[2] // 128
        per = next(d for d in (11, 4, 2, 1) if count % d == 0)
        spread = jnp.broadcast_to(gains[a // 3], (128, feats)).T

        def tile(i):
            for piece in range(per):
                at = pl.ds(pl.multiple_of((i * per + piece) * 128, 128), 128)
                block = raw[a, :, at]
                if a % 3 != 2:
                    block = block * spread
                cut[a, at, :] = block.astype(jnp.bfloat16).T

        loop(0, count // per, tile)
        own = pl.ds(pl.multiple_of(me * rows, rows), rows)
        served[a][core, :, mine] = cut[a, own, :]

    def block_copy(a, g, i):
        to = planes[g] * inner + lax.rem(col + i, inner)
        return pltpu.make_async_remote_copy(
            src_ref=cut.at[a, pl.ds(pl.multiple_of(to * rows, rows), rows), :],
            dst_ref=served[a].at[core, :, mine],
            send_sem=send_sem.at[a, g * inner + i],
            recv_sem=recv_sem.at[a, g * inner + i],
            device_id={"fs": to},
            device_id_type=pl.DeviceIdType.MESH,
        )

    def first(g):
        return 1 if g == 0 else 0

    def send(a, g, lo=None, hi=None):
        lo = first(g) if lo is None else lo
        hi = inner if hi is None else hi
        loop(lo, hi, lambda i: block_copy(a, g, i).start())

    def pass_copy(a, g):
        spot = served[a].at[core, :, columns(g)]
        return pltpu.make_async_remote_copy(
            src_ref=spot,
            dst_ref=spot,
            send_sem=pass_send.at[a, g],
            recv_sem=pass_recv.at[a, g],
            device_id={"tp": 1 - core},
            device_id_type=pl.DeviceIdType.MESH,
        )

    def arrive(a, *groups):
        for g in groups:
            loop(first(g), inner, lambda i, g=g: block_copy(a, g, i).wait_recv())
            pass_copy(a, g).start()

    def complete(a, *groups):
        for g in groups:
            pass_copy(a, g).wait_recv()

    waiting = [(a, g, i) for a in (3, 4, 5) for g in (2, 3) for i in range(inner)]

    def fill(count):
        batch, waiting[:] = waiting[:count], waiting[count:]
        while batch:
            a, g, i = batch[0]
            run = [x for x in batch if x[:2] == (a, g)]
            batch = batch[len(run):]
            send(a, g, i, i + len(run))

    def remote(src, dst, sends, recvs, at, to):
        return pltpu.make_async_remote_copy(
            src_ref=src,
            dst_ref=dst,
            send_sem=sends.at[at],
            recv_sem=recvs.at[at],
            device_id={"fs": to},
            device_id_type=pl.DeviceIdType.MESH,
        )

    def plane_copies(half, g):
        copies = []
        for k in range(1, inner):
            to = lax.rem(col + k, inner)
            copies.append(
                remote(
                    part.at[half, to, :, :, columns(g)],
                    plane_in.at[half, k - 1, :, :, columns(g)],
                    plane_send, plane_recv, (half, g, k), row * inner + to,
                )
            )
        return copies

    def line_copies(half, g):
        copies = []
        for k in range(1, outer):
            to = lax.rem(row + k, outer)
            copies.append(
                remote(
                    plane_sum.at[half, to, :, columns(g)],
                    line_in.at[half, k - 1, :, columns(g)],
                    line_send, line_recv, (half, g, k), to * inner + col,
                )
            )
        return copies

    def spread_line():
        spot = middle.at[col, row]
        return [
            remote(spot, spot, spread_send, spread_recv, (0, k),
                   lax.rem(row + k, outer) * inner + col)
            for k in range(1, outer)
        ]

    def spread_plane():
        spot = middle.at[col]
        return [
            remote(spot, spot, spread_send, spread_recv, (1, k),
                   row * inner + lax.rem(col + k, inner))
            for k in range(1, inner)
        ]

    def normalize_rows(pick):
        def one(i):
            wide = pick(i).astype(jnp.float32)
            scale = lax.rsqrt(jnp.mean(wide * wide, axis=-1, keepdims=True) + 1e-06)
            at = pl.ds(pl.multiple_of(i * outer * keep, outer * keep), outer * keep)
            normed[at, :] = (wide * scale).astype(jnp.bfloat16).reshape(outer * keep, depth)

        loop(0, inner, one)

    def expand(g, u):
        left = normed[...]
        dims = (((1,), (1,)), ((), ()))
        gate = lax.dot_general(
            left, served[g][...].reshape(-1, depth), dims, preferred_element_type=jnp.float32
        )
        up = lax.dot_general(
            left, served[u][...].reshape(-1, depth), dims, preferred_element_type=jnp.float32
        )
        hidden[...] = (gate / (1.0 + jnp.exp(-gate)) * up).astype(jnp.bfloat16)

    def contract(d, half, g):
        right = served[d][:, :, columns(g)].reshape(-1, band)
        value = jnp.dot(hidden[...], right, preferred_element_type=jnp.float32)
        part[half, :, :, :, columns(g)] = value.astype(jnp.bfloat16).reshape(
            inner, outer, keep, band
        )

    def sum_plane(half, g):
        total = part[half, col, :, :, columns(g)].astype(jnp.float32)
        for k in range(inner - 1):
            total += plane_in[half, k, :, :, columns(g)].astype(jnp.float32)
        plane_sum[half, :, :, columns(g)] = total.astype(jnp.bfloat16)

    def sum_line(half):
        total = plane_sum[half, row].astype(jnp.float32)
        for k in range(outer - 1):
            total += line_in[half, k].astype(jnp.float32)
        return total

    def start(copies):
        for copy in copies:
            copy.start()

    def receive(copies):
        for copy in copies:
            copy.wait_recv()

    def contract_near(d, half):
        for g in (0, 1):
            complete(d, g)
            contract(d, half, g)
            start(plane_copies(half, g))

    def contract_far(d, half):
        for g in (2, 3):
            arrive(d, g)
            complete(d, g)
            contract(d, half, g)
            start(plane_copies(half, g))

    def hand_plane(half, *groups):
        for g in groups:
            receive(plane_copies(half, g))
            sum_plane(half, g)
            start(line_copies(half, g))

    barrier = pltpu.get_barrier_semaphore()
    loop(
        1,
        n,
        lambda j: pl.semaphore_signal(
            barrier, inc=1, device_id={"fs": lax.rem(me + j, n)},
            device_id_type=pl.DeviceIdType.MESH,
        ),
    )
    pl.semaphore_signal(
        barrier, inc=1, device_id={"tp": 1 - core}, device_id_type=pl.DeviceIdType.MESH
    )
    for copy in side_loads[:2]:
        copy.start()
    for a in range(6):
        load(a).start()
    side_loads[2].start()
    for copy in side_loads[:2]:
        copy.wait()
    cast(0)
    cast(1)
    pl.semaphore_wait(barrier, n)
    for a in (0, 1, 2):
        if a == 2:
            cast(a)
        for g in (2, 3, 1, 0):
            send(a, g)
    for a in (3, 4, 5):
        cast(a)
        for g in (1, 0):
            send(a, g)
    fill(early)
    side_loads[2].wait()
    normalize_rows(lambda c: tokens_ref[:, c])
    for a in (0, 1, 2):
        arrive(a, 0, 1)
    for a in (0, 1):
        arrive(a, 2, 3)
    for a in (0, 1):
        complete(a, 0, 1, 2, 3)
    expand(0, 1)
    contract_near(2, 0)
    hand_plane(0, 0, 1)
    for a in (3, 4, 5):
        arrive(a, 0, 1)
    contract_far(2, 0)
    hand_plane(0, 2, 3)
    fill(mid)
    for g in range(outer):
        receive(line_copies(0, g))
    own = tokens_ref[row, col].astype(jnp.float32) + 0.5 * sum_line(0)
    middle[col, row] = own.astype(jnp.bfloat16)
    start(spread_line())
    fill(late)
    receive(spread_line())
    start(spread_plane())
    fill(len(waiting))
    receive(spread_plane())
    normalize_rows(lambda c: middle[c])
    for a in (3, 4):
        arrive(a, 2, 3)
    for a in (3, 4):
        complete(a, 0, 1, 2, 3)
    expand(3, 4)
    contract_near(5, 1)
    hand_plane(1, 0, 1)
    contract_far(5, 1)
    hand_plane(1, 2, 3)
    for g in range(outer):
        receive(line_copies(1, g))
    last = middle[col, row].astype(jnp.float32) + 0.5 * sum_line(1)
    mixed_ref[...] = last.astype(jnp.bfloat16)

    for a in range(6):
        for g in range(outer):
            pass_copy(a, g).wait_send()
            loop(first(g), inner, lambda i, a=a, g=g: block_copy(a, g, i).wait_send())
    for half in (0, 1):
        for g in range(outer):
            for copy in plane_copies(half, g) + line_copies(half, g):
                copy.wait_send()
    for copy in spread_line() + spread_plane():
        copy.wait_send()


def hand_on(*refs):
    sems = refs[-1]
    half = len(refs) // 2
    copies = [
        pltpu.make_async_copy(source, target, sems.at[i])
        for i, (source, target) in enumerate(zip(refs[:half], refs[half : 2 * half]))
    ]
    for copy in copies:
        copy.start()
    for copy in copies:
        copy.wait()


def fused_shards(tokens, gain_first, gate_first, up_first, down_first,
                 gain_second, gate_second, up_second, down_second):
    n = lax.axis_size("fs")
    tp = lax.axis_size("tp")
    inner = math.isqrt(n)
    outer = n // inner
    feats, units = gate_first.shape
    rows = units // n
    plen, depth = tokens.shape[1], tokens.shape[2]
    keep = plen // n
    bf16, f32 = jnp.bfloat16, jnp.float32
    shuffled = tokens[0].reshape(outer, inner, keep, depth)
    anywhere = pl.BlockSpec(memory_space=pl.ANY)
    hbm = pl.BlockSpec(memory_space=pltpu.HBM)
    vmem = pl.BlockSpec(memory_space=pltpu.VMEM)
    served_shape = (tp, rows, depth)
    hid = tp * rows
    dma = pltpu.SemaphoreType.DMA
    results = pl.pallas_call(
        functools.partial(step_kernel, n, inner, 8, 3, 3),
        out_shape=(pltpu.VMEM((keep, depth), bf16),)
        + (pltpu.VMEM(served_shape, bf16),) * 6,
        in_specs=[hbm] * 9,
        out_specs=(vmem,) * 7,
        scratch_shapes=[
            pltpu.VMEM((6, feats, units), f32),
            pltpu.VMEM((6, units, feats), bf16),
            pltpu.VMEM((outer, inner, keep, depth), bf16),
            pltpu.VMEM((2, 1, feats), f32),
            pltpu.VMEM((plen, depth), bf16),
            pltpu.VMEM((plen, hid), bf16),
            pltpu.VMEM((inner, outer, keep, depth), bf16),
            pltpu.VMEM((2, inner, outer, keep, depth), bf16),
            pltpu.VMEM((2, inner - 1, outer, keep, depth), bf16),
            pltpu.VMEM((2, outer, keep, depth), bf16),
            pltpu.VMEM((2, outer - 1, keep, depth), bf16),
            dma((6,)),
            dma((3,)),
            dma((6, n)),
            dma((6, n)),
            dma((6, outer)),
            dma((6, outer)),
            dma((2, outer, inner)),
            dma((2, outer, inner)),
            dma((2, outer, outer)),
            dma((2, outer, outer)),
            dma((2, outer)),
            dma((2, outer)),
        ],
        compiler_params=pltpu.CompilerParams(
            has_side_effects=True, collective_id=0, vmem_limit_bytes=40 * 1024 * 1024
        ),
    )(
        *(
            pltpu.with_memory_space_constraint(x, pltpu.HBM)
            for x in (
                shuffled,
                gain_first.reshape(1, feats),
                gain_second.reshape(1, feats),
                gate_first,
                up_first,
                down_first,
                gate_second,
                up_second,
                down_second,
            )
        )
    )
    outs = pl.pallas_call(
        hand_on,
        out_shape=(jax.ShapeDtypeStruct((keep, depth), bf16),)
        + (jax.ShapeDtypeStruct(served_shape, bf16),) * 6,
        in_specs=[anywhere] * 7,
        out_specs=(anywhere,) * 7,
        scratch_shapes=[dma((7,))],
        compiler_params=pltpu.CompilerParams(vmem_limit_bytes=1024 * 1024),
    )(*results)
    return (outs[0][None],) + tuple(outs[1:])


def fits(mesh, tokens, gate):
    n, tp = mesh.shape["fs"], mesh.shape["tp"]
    inner = math.isqrt(n)
    depth, hidden = gate.shape
    plen = tokens.shape[1]
    if tp != 2 or inner != 4 or n != inner * inner:
        return False
    if depth % (n * 128) or hidden % (tp * n * 16):
        return False
    if (hidden // tp) % 128 or plen % (n * 16) or tokens.shape[0] != tp:
        return False
    local = depth // n * (hidden // tp)
    need = local * 6 * 4 + local * 6 * 2
    need += plen * depth * 2 * 8 + plen * (hidden // n) * 12
    return need < 34 * 1024 * 1024


def solution(mesh):
    def run(body):
        return jax.shard_map(
            body,
            mesh=mesh,
            in_specs=(
                P("tp", None, None),
                P("fs"),
                P("fs", "tp"),
                P("fs", "tp"),
                P("fs", "tp"),
                P("fs"),
                P("fs", "tp"),
                P("fs", "tp"),
                P("fs", "tp"),
            ),
            out_specs=(
                P("tp", "fs", None),
                P(None, "fs", None),
                P(None, "fs", None),
                P(None, "fs", None),
                P(None, "fs", None),
                P(None, "fs", None),
                P(None, "fs", None),
            ),
            check_vma=False,
        )

    def step(*args):
        return run(fused_shards if fits(mesh, args[0], args[2]) else shards)(*args)

    return step
```

time: 169 us -> 142 us (0.84)
  Pallas kernels: 168 us -> 141 us
    pallas_call x2, Pallas kernels: 168 us -> 141 us  [the longest x1 138 us: fused_shards(): pl.pallas_call(functools.partial(step_kernel, n, inner, 8, 3, 3), out_sha...]
where the time goes in v1:
time: 142 us
  Pallas kernels  141 us (99%)
    pallas_call x1, Pallas kernels, fused_shards(): pl.pallas_call(functools.partial(step_kernel, n, inner, 8, 3, 3), out_sha...  138 us
    pallas_call x1, Pallas kernels, fused_shards(): pl.pallas_call(hand_on, out_shape=(jax.ShapeDtypeStruct((keep, depth), bf...  3.48 us

profile of v1, /device:TPU:0, one launch (start us, length us, event | category | flops | bytes accessed | tf_op | source)
XLA Modules:
  0.0 141.8 jit_solution(10132887456274202160)
XLA Ops:
  0.6 137.7 %shard_map.144 = (bf16[16,2048]{1,0:T(8,128)(2,1)S(1)}, bf16[2,176,2048]{2,1,0:T(8,128)(2,1)S(1)}, bf16[2,176,2048]{2,1,0:T(8,128)(2,1)S(1)}, bf16[2,176,2048]{2...) custom-call(bf16[4,4,16,2048]{3,2,1,0:T(8,128)(2,1)} %bitcast.4, ...), custom_call_target="tpu_custom_call" | custom-call | tf_op jit(solution)/shard_map/pallas_call | solution.py:464
  138.3 3.5 %shard_map.145 = (bf16[16,2048]{1,0:T(8,128)(2,1)}, bf16[2,176,2048]{2,1,0:T(8,128)(2,1)}, bf16[2,176,2048]{2,1,0:T(8,128)(2,1)}, bf16[2,176,2048]{2,1,0:T(8,128...) custom-call(bf16[16,2048]{1,0:T(8,128)(2,1)S(1)} %get-tuple-element.21.refs_0_, ...), custom_call_target="tpu_custom_call" | custom-call | tf_op jit(solution)/shard_map/pallas_call | solution.py:514

commit v2 on v1

--- a/solution.py
+++ b/solution.py
@@ -90,9 +90,6 @@
 def step_kernel(
     n,
     inner,
-    early,
-    mid,
-    late,
     tokens_hbm,
     gain_one_hbm,
     gain_two_hbm,
@@ -117,21 +114,30 @@
     hidden,
     middle,
     part,
+    inbox,
     plane_in,
     plane_sum,
-    line_in,
+    twin_in,
+    summed,
+    across,
     load_sem,
     side_sem,
     send_sem,
     recv_sem,
     pass_send,
     pass_recv,
+    part_send,
+    part_recv,
     plane_send,
     plane_recv,
-    line_send,
-    line_recv,
+    twin_send,
+    twin_recv,
+    cross_send,
+    cross_recv,
     spread_send,
     spread_recv,
+    last_recv,
+    last_pass,
 ):
     outer = n // inner
     me = lax.axis_index("fs")
@@ -143,13 +149,16 @@
     rows = o0.shape[1]
     feats = cut.shape[2]
     depth = normed.shape[1]
+    side = n // 2
+    half = me // side
+    spot = lax.rem(me, side)
     keep = tokens_ref.shape[2]
     band = depth // outer
     mine = pl.ds(pl.multiple_of(me * feats, feats), feats)
     planes = (row, row + 1 - 2 * lax.rem(row, 2), outer - 1 - row, lax.rem(row + 2, outer))
 
-    def columns(g):
-        return pl.ds(pl.multiple_of(planes[g] * band, band), band)
+    def columns(b):
+        return pl.ds(pl.multiple_of(b * band, band), band)
 
     def load(a):
         return pltpu.make_async_copy(weights[a], raw.at[a], load_sem.at[a])
@@ -178,115 +187,163 @@
         own = pl.ds(pl.multiple_of(me * rows, rows), rows)
         served[a][core, :, mine] = cut[a, own, :]
 
-    def block_copy(a, g, i):
+    def block_copy(a, g, i, recvs=None):
         to = planes[g] * inner + lax.rem(col + i, inner)
         return pltpu.make_async_remote_copy(
             src_ref=cut.at[a, pl.ds(pl.multiple_of(to * rows, rows), rows), :],
             dst_ref=served[a].at[core, :, mine],
-            send_sem=send_sem.at[a, g * inner + i],
-            recv_sem=recv_sem.at[a, g * inner + i],
+            send_sem=send_sem.at[a],
+            recv_sem=recv_sem.at[a, row] if recvs is None else recvs.at[i],
             device_id={"fs": to},
             device_id_type=pl.DeviceIdType.MESH,
         )
 
-    def first(g):
-        return 1 if g == 0 else 0
-
-    def send(a, g, lo=None, hi=None):
-        lo = first(g) if lo is None else lo
-        hi = inner if hi is None else hi
-        loop(lo, hi, lambda i: block_copy(a, g, i).start())
-
-    def pass_copy(a, g):
-        spot = served[a].at[core, :, columns(g)]
+    def send(a, *groups):
+        for g in groups:
+            loop(1 if g == 0 else 0, inner, lambda i, g=g: block_copy(a, g, i).start())
+
+    def send_last(*groups):
+        for g in groups:
+            loop(0, inner, lambda i, g=g: block_copy(5, g, i, last_recv).start())
+
+    def counted(ref, sends, recvs):
         return pltpu.make_async_remote_copy(
-            src_ref=spot,
-            dst_ref=spot,
-            send_sem=pass_send.at[a, g],
-            recv_sem=pass_recv.at[a, g],
+            src_ref=ref,
+            dst_ref=ref,
+            send_sem=sends,
+            recv_sem=recvs,
             device_id={"tp": 1 - core},
             device_id_type=pl.DeviceIdType.MESH,
         )
 
-    def arrive(a, *groups):
-        for g in groups:
-            loop(first(g), inner, lambda i, g=g: block_copy(a, g, i).wait_recv())
-            pass_copy(a, g).start()
-
-    def complete(a, *groups):
-        for g in groups:
-            pass_copy(a, g).wait_recv()
-
-    waiting = [(a, g, i) for a in (3, 4, 5) for g in (2, 3) for i in range(inner)]
-
-    def fill(count):
-        batch, waiting[:] = waiting[:count], waiting[count:]
-        while batch:
-            a, g, i = batch[0]
-            run = [x for x in batch if x[:2] == (a, g)]
-            batch = batch[len(run):]
-            send(a, g, i, i + len(run))
-
-    def remote(src, dst, sends, recvs, at, to):
+    def pass_slot(a, b):
+        return a + first_slot[a] + (b if a % 3 == 2 else 0)
+
+    first_slot = (0, 0, 0, outer - 1, outer - 1, outer - 1)
+
+    def pass_copy(a, b):
+        return counted(
+            served[a].at[core, :, columns(b)], pass_send.at[0], pass_recv.at[pass_slot(a, b)]
+        )
+
+    def arrive(a, b, blocks=inner):
+        at = pl.ds(0, blocks * feats)
+        counted(served[a].at[core, :, at], send_sem.at[a], recv_sem.at[a, b]).wait_recv()
+        pass_copy(a, b).start()
+
+    def arrive_near(a):
+        arrive(a, row, inner - 1)
+        arrive(a, planes[1])
+
+    def complete(a, b=None):
+        at = slice(None) if b is None else columns(b)
+        slot = pass_recv.at[pass_slot(a, 0 if b is None else b)]
+        counted(served[a].at[core, :, at], pass_send.at[0], slot).wait_recv()
+
+    def remote(src, dst, sends, recvs, to):
         return pltpu.make_async_remote_copy(
             src_ref=src,
             dst_ref=dst,
-            send_sem=sends.at[at],
-            recv_sem=recvs.at[at],
+            send_sem=sends,
+            recv_sem=recvs,
             device_id={"fs": to},
             device_id_type=pl.DeviceIdType.MESH,
         )
 
-    def plane_copies(half, g):
-        copies = []
+    level = lax.rem(row, 2)
+    twin = lax.rem(spot + inner, side)
+    twin_id = half * side + twin
+
+    def start_part(at, b):
+        def one(k):
+            to = lax.rem(spot + k, side)
+            remote(
+                part.at[1, to // inner, lax.rem(to, inner), :, :, at],
+                inbox.at[k - 1, :, :, at],
+                part_send.at[0],
+                part_recv.at[b],
+                half * side + to,
+            ).start()
+
+        loop(1, side, one)
+
+    def start_plane(block, b):
         for k in range(1, inner):
             to = lax.rem(col + k, inner)
-            copies.append(
-                remote(
-                    part.at[half, to, :, :, columns(g)],
-                    plane_in.at[half, k - 1, :, :, columns(g)],
-                    plane_send, plane_recv, (half, g, k), row * inner + to,
-                )
-            )
-        return copies
-
-    def line_copies(half, g):
-        copies = []
-        for k in range(1, outer):
-            to = lax.rem(row + k, outer)
-            copies.append(
-                remote(
-                    plane_sum.at[half, to, :, columns(g)],
-                    line_in.at[half, k - 1, :, columns(g)],
-                    line_send, line_recv, (half, g, k), to * inner + col,
-                )
-            )
-        return copies
+            remote(
+                part.at[block, :, to, :, :, columns(b)],
+                plane_in.at[block, k - 1, :, :, :, columns(b)],
+                plane_send.at[block],
+                plane_recv.at[block, b],
+                row * inner + to,
+            ).start()
+
+    def hand_plane(block, b):
+        at = columns(b)
+        counted(
+            plane_in.at[block, :, :, :, :, at], plane_send.at[block], plane_recv.at[block, b]
+        ).wait_recv()
+        total = part[block, :, col, :, :, at].astype(jnp.float32)
+        for k in range(inner - 1):
+            total += plane_in[block, k, :, :, :, at].astype(jnp.float32)
+        plane_sum[block, :, :, :, at] = total.astype(jnp.bfloat16)
+        remote(
+            plane_sum.at[block, 1 - level, :, :, at],
+            twin_in.at[block, :, :, at],
+            twin_send.at[block],
+            twin_recv.at[block, b],
+            twin_id,
+        ).start()
+
+    def hand_twin(block, b):
+        at = columns(b)
+        counted(
+            twin_in.at[block, :, :, at], twin_send.at[block], twin_recv.at[block, b]
+        ).wait_recv()
+        total = plane_sum[block, level, :, :, at].astype(jnp.float32)
+        total += twin_in[block, :, :, at].astype(jnp.float32)
+        summed[block, :, :, at] = total.astype(jnp.bfloat16)
+
+    def cross_copy(block, b):
+        if block == 0:
+            out, into = summed.at[0], across.at[0]
+        else:
+            out, into = summed.at[1, pl.ds(1 - half, 1)], across.at[1, pl.ds(1 - half, 1)]
+        return remote(
+            out.at[:, :, columns(b)],
+            into.at[:, :, columns(b)],
+            cross_send.at[block],
+            cross_recv.at[block],
+            lax.rem(me + side, n),
+        )
+
+    def receive_cross(block):
+        ref = across.at[0] if block == 0 else across.at[1, half]
+        counted(ref, cross_send.at[block], cross_recv.at[block]).wait_recv()
 
     def spread_line():
-        spot = middle.at[col, row]
-        return [
-            remote(spot, spot, spread_send, spread_recv, (0, k),
-                   lax.rem(row + k, outer) * inner + col)
-            for k in range(1, outer)
-        ]
-
-    def spread_plane():
-        spot = middle.at[col]
-        return [
-            remote(spot, spot, spread_send, spread_recv, (1, k),
-                   row * inner + lax.rem(col + k, inner))
-            for k in range(1, inner)
-        ]
+        return remote(
+            middle.at[spot], middle.at[spot], spread_send.at[0], spread_recv.at[0],
+            twin_id,
+        )
+
+    def spread_plane(at):
+        for k in range(1, inner):
+            to = row * inner + lax.rem(col + k, inner)
+            remote(
+                middle.at[at], middle.at[at], spread_send.at[1], spread_recv.at[1], to
+            ).start()
+
+    around = middle.at[pl.ds(0, 2 * (inner - 1))]
 
     def normalize_rows(pick):
         def one(i):
             wide = pick(i).astype(jnp.float32)
             scale = lax.rsqrt(jnp.mean(wide * wide, axis=-1, keepdims=True) + 1e-06)
-            at = pl.ds(pl.multiple_of(i * outer * keep, outer * keep), outer * keep)
-            normed[at, :] = (wide * scale).astype(jnp.bfloat16).reshape(outer * keep, depth)
-
-        loop(0, inner, one)
+            at = pl.ds(pl.multiple_of(i * 2 * keep, 2 * keep), 2 * keep)
+            normed[at, :] = (wide * scale).astype(jnp.bfloat16).reshape(2 * keep, depth)
+
+        loop(0, side, one)
 
     def expand(g, u):
         left = normed[...]
@@ -299,52 +356,55 @@
         )
         hidden[...] = (gate / (1.0 + jnp.exp(-gate)) * up).astype(jnp.bfloat16)
 
-    def contract(d, half, g):
-        right = served[d][:, :, columns(g)].reshape(-1, band)
+    def product(d, block, at):
+        width = at.size
+        right = served[d][:, :, at].reshape(-1, width)
         value = jnp.dot(hidden[...], right, preferred_element_type=jnp.float32)
-        part[half, :, :, :, columns(g)] = value.astype(jnp.bfloat16).reshape(
-            inner, outer, keep, band
-        )
-
-    def sum_plane(half, g):
-        total = part[half, col, :, :, columns(g)].astype(jnp.float32)
-        for k in range(inner - 1):
-            total += plane_in[half, k, :, :, columns(g)].astype(jnp.float32)
-        plane_sum[half, :, :, columns(g)] = total.astype(jnp.bfloat16)
-
-    def sum_line(half):
-        total = plane_sum[half, row].astype(jnp.float32)
-        for k in range(outer - 1):
-            total += line_in[half, k].astype(jnp.float32)
-        return total
-
-    def start(copies):
-        for copy in copies:
-            copy.start()
-
-    def receive(copies):
-        for copy in copies:
-            copy.wait_recv()
-
-    def contract_near(d, half):
-        for g in (0, 1):
-            complete(d, g)
-            contract(d, half, g)
-            start(plane_copies(half, g))
-
-    def contract_far(d, half):
-        for g in (2, 3):
-            arrive(d, g)
-            complete(d, g)
-            contract(d, half, g)
-            start(plane_copies(half, g))
-
-    def hand_plane(half, *groups):
-        for g in groups:
-            receive(plane_copies(half, g))
-            sum_plane(half, g)
-            start(line_copies(half, g))
-
+        part[block, :, :, :, :, at] = value.astype(jnp.bfloat16).reshape(
+            2, inner, 2, keep, width
+        )
+
+    def contract(d, block, b):
+        complete(d, b)
+        product(d, block, columns(b))
+
+    def last_at(i):
+        source = far_mid * inner + lax.rem(col + inner - i, inner)
+        return pl.ds(pl.multiple_of(source * feats, feats), feats)
+
+    def last_copy(i):
+        return counted(
+            served[5].at[core, :, last_at(i)], pass_send.at[0], last_pass.at[i]
+        )
+
+    def arrive_last(i):
+        counted(
+            served[5].at[core, :, last_at(i)], send_sem.at[5], last_recv.at[i]
+        ).wait_recv()
+        last_copy(i).start()
+
+    def contract_last(i):
+        last_copy(i).wait_recv()
+        product(5, 1, last_at(i))
+        start_part(last_at(i), far_mid)
+
+    def hand_part(b):
+        at = columns(b)
+        counted(inbox.at[:, :, :, at], part_send.at[0], part_recv.at[b]).wait_recv()
+        total = part[1, level, col, :, :, at].astype(jnp.float32)
+        for k in range(side - 1):
+            total += inbox[k, :, :, at].astype(jnp.float32)
+        summed[1, :, :, at] = total.astype(jnp.bfloat16)
+        cross_copy(1, b).start()
+
+    near = (half * (outer // 2), half * (outer // 2) + 1)
+    far_end = (outer - 1) * (1 - half)
+    far_mid = outer // 2 - half
+
+    ends = jnp.logical_or(row == 0, row == outer - 1)
+    for copy in side_loads[:2]:
+        copy.start()
+    load(0).start()
     barrier = pltpu.get_barrier_semaphore()
     loop(
         1,
@@ -357,77 +417,135 @@
     pl.semaphore_signal(
         barrier, inc=1, device_id={"tp": 1 - core}, device_id_type=pl.DeviceIdType.MESH
     )
-    for copy in side_loads[:2]:
-        copy.start()
-    for a in range(6):
+    for a in range(1, 6):
         load(a).start()
     side_loads[2].start()
     for copy in side_loads[:2]:
         copy.wait()
+    at_end = pl.when(ends)
+    at_mid = pl.when(jnp.logical_not(ends))
     cast(0)
-    cast(1)
     pl.semaphore_wait(barrier, n)
-    for a in (0, 1, 2):
-        if a == 2:
-            cast(a)
-        for g in (2, 3, 1, 0):
-            send(a, g)
+    at_mid(lambda: send(0, 2, 3, 1, 0))
+    at_end(lambda: send(0, 1, 0))
+    for a in (1, 2):
+        cast(a)
+        at_mid(lambda a=a: send(a, 2, 3, 1, 0))
+        at_end(lambda a=a: send(a, 1, 0))
     for a in (3, 4, 5):
         cast(a)
-        for g in (1, 0):
-            send(a, g)
-    fill(early)
+
+    @at_mid
+    def _():
+        for a in (3, 4):
+            send(a, 2, 1, 0)
+        send(3, 3)
+
+    @at_end
+    def _():
+        for a in (0, 1):
+            send(a, 2, 3)
+        for a in (3, 4):
+            send(a, 1, 0)
+        send(2, 2, 3)
+
     side_loads[2].wait()
-    normalize_rows(lambda c: tokens_ref[:, c])
+    normalize_rows(lambda q: tokens_ref[:, q])
     for a in (0, 1, 2):
-        arrive(a, 0, 1)
+        arrive_near(a)
     for a in (0, 1):
-        arrive(a, 2, 3)
+        arrive(a, far_end)
+        arrive(a, far_mid)
     for a in (0, 1):
-        complete(a, 0, 1, 2, 3)
+        complete(a)
     expand(0, 1)
-    contract_near(2, 0)
-    hand_plane(0, 0, 1)
-    for a in (3, 4, 5):
-        arrive(a, 0, 1)
-    contract_far(2, 0)
-    hand_plane(0, 2, 3)
-    fill(mid)
-    for g in range(outer):
-        receive(line_copies(0, g))
-    own = tokens_ref[row, col].astype(jnp.float32) + 0.5 * sum_line(0)
-    middle[col, row] = own.astype(jnp.bfloat16)
-    start(spread_line())
-    fill(late)
-    receive(spread_line())
-    start(spread_plane())
-    fill(len(waiting))
-    receive(spread_plane())
-    normalize_rows(lambda c: middle[c])
+    for b in near:
+        contract(2, 0, b)
+        start_plane(0, b)
+    arrive(2, far_end)
+    contract(2, 0, far_end)
+    start_plane(0, far_end)
+    for b in near:
+        hand_plane(0, b)
+    arrive(2, far_mid)
+    contract(2, 0, far_mid)
+    start_plane(0, far_mid)
+    hand_plane(0, far_end)
+    for b in near:
+        hand_twin(0, b)
+        cross_copy(0, b).start()
+    hand_plane(0, far_mid)
+    for b in (far_end, far_mid):
+        hand_twin(0, b)
+        cross_copy(0, b).start()
+    at_mid(lambda: send(4, 3))
     for a in (3, 4):
-        arrive(a, 2, 3)
+        arrive_near(a)
+    receive_cross(0)
+    branch = summed[0].astype(jnp.float32) + across[0].astype(jnp.float32)
+    own = tokens_ref[:, spot].astype(jnp.float32) + 0.5 * branch
+    middle[spot] = own.astype(jnp.bfloat16)
+    spread_line().start()
+    spread_plane(spot)
+    send(5, 1, 0)
+    at_mid(lambda: send_last(3, 2))
+
+    @at_end
+    def _():
+        for g in (3, 2):
+            send(3, g)
+            send(4, g)
+
+    spread_line().wait_recv()
+    spread_plane(twin)
     for a in (3, 4):
-        complete(a, 0, 1, 2, 3)
+        arrive(a, far_end)
+        arrive(a, far_mid)
+    at_end(lambda: send(5, 2, 3))
+    arrive_near(5)
+    counted(around, spread_send.at[1], spread_recv.at[1]).wait_recv()
+    normalize_rows(lambda q: middle[q])
+    for a in (3, 4):
+        complete(a)
     expand(3, 4)
-    contract_near(5, 1)
-    hand_plane(1, 0, 1)
-    contract_far(5, 1)
-    hand_plane(1, 2, 3)
-    for g in range(outer):
-        receive(line_copies(1, g))
-    last = middle[col, row].astype(jnp.float32) + 0.5 * sum_line(1)
+    for b in near:
+        contract(5, 1, b)
+        start_plane(1, b)
+    arrive(5, far_end)
+    contract(5, 1, far_end)
+    start_part(columns(far_end), far_end)
+    for b in near:
+        hand_plane(1, b)
+    arrive_last(0)
+    for i in range(1, inner):
+        arrive_last(i)
+        contract_last(i - 1)
+    for b in near:
+        hand_twin(1, b)
+        cross_copy(1, b).start()
+    contract_last(inner - 1)
+    hand_part(far_end)
+    hand_part(far_mid)
+    for a in range(6):
+        spent = cut.at[a, pl.ds(0, (n - 1) * rows), :]
+        counted(spent, send_sem.at[a], recv_sem.at[a, 0]).wait_send()
+        counted(served[a].at[core], pass_send.at[0], pass_recv.at[0]).wait_send()
+    spread_line().wait_send()
+    counted(around, spread_send.at[1], spread_recv.at[1]).wait_send()
+    two = pl.ds(0, 2 * band)
+    counted(inbox.at[:, :, :, two], part_send.at[0], part_recv.at[0]).wait_send()
+    for block, at in ((0, slice(None)), (1, two)):
+        spent = plane_in.at[block, :, :, :, :, at]
+        counted(spent, plane_send.at[block], plane_recv.at[block, 0]).wait_send()
+        counted(
+            twin_in.at[block, :, :, at], twin_send.at[block], twin_recv.at[block, 0]
+        ).wait_send()
+    receive_cross(1)
+    branch = summed[1, half].astype(jnp.float32) + across[1, half].astype(jnp.float32)
+    last = middle[spot, half].astype(jnp.float32) + 0.5 * branch
     mixed_ref[...] = last.astype(jnp.bfloat16)
-
-    for a in range(6):
-        for g in range(outer):
-            pass_copy(a, g).wait_send()
-            loop(first(g), inner, lambda i, a=a, g=g: block_copy(a, g, i).wait_send())
-    for half in (0, 1):
-        for g in range(outer):
-            for copy in plane_copies(half, g) + line_copies(half, g):
-                copy.wait_send()
-    for copy in spread_line() + spread_plane():
-        copy.wait_send()
+    counted(summed.at[0], cross_send.at[0], cross_recv.at[0]).wait_send()
+    counted(summed.at[1, 0], cross_send.at[1], cross_recv.at[1]).wait_send()
 
 
 def hand_on(*refs):
@@ -454,7 +572,7 @@
     plen, depth = tokens.shape[1], tokens.shape[2]
     keep = plen // n
     bf16, f32 = jnp.bfloat16, jnp.float32
-    shuffled = tokens[0].reshape(outer, inner, keep, depth)
+    shuffled = tokens[0].reshape(2, n // 2, keep, depth)
     anywhere = pl.BlockSpec(memory_space=pl.ANY)
     hbm = pl.BlockSpec(memory_space=pltpu.HBM)
     vmem = pl.BlockSpec(memory_space=pltpu.VMEM)
@@ -462,7 +580,7 @@
     hid = tp * rows
     dma = pltpu.SemaphoreType.DMA
     results = pl.pallas_call(
-        functools.partial(step_kernel, n, inner, 8, 3, 3),
+        functools.partial(step_kernel, n, inner),
         out_shape=(pltpu.VMEM((keep, depth), bf16),)
         + (pltpu.VMEM(served_shape, bf16),) * 6,
         in_specs=[hbm] * 9,
@@ -470,27 +588,36 @@
         scratch_shapes=[
             pltpu.VMEM((6, feats, units), f32),
             pltpu.VMEM((6, units, feats), bf16),
-            pltpu.VMEM((outer, inner, keep, depth), bf16),
+            pltpu.VMEM((2, n // 2, keep, depth), bf16),
             pltpu.VMEM((2, 1, feats), f32),
             pltpu.VMEM((plen, depth), bf16),
             pltpu.VMEM((plen, hid), bf16),
-            pltpu.VMEM((inner, outer, keep, depth), bf16),
-            pltpu.VMEM((2, inner, outer, keep, depth), bf16),
-            pltpu.VMEM((2, inner - 1, outer, keep, depth), bf16),
-            pltpu.VMEM((2, outer, keep, depth), bf16),
-            pltpu.VMEM((2, outer - 1, keep, depth), bf16),
+            pltpu.VMEM((n // 2, 2, keep, depth), bf16),
+            pltpu.VMEM((2, 2, inner, 2, keep, depth), bf16),
+            pltpu.VMEM((n // 2 - 1, 2, keep, depth), bf16),
+            pltpu.VMEM((2, inner - 1, 2, 2, keep, depth), bf16),
+            pltpu.VMEM((2, 2, 2, keep, depth), bf16),
+            pltpu.VMEM((2, 2, keep, depth), bf16),
+            pltpu.VMEM((2, 2, keep, depth), bf16),
+            pltpu.VMEM((2, 2, keep, depth), bf16),
             dma((6,)),
             dma((3,)),
-            dma((6, n)),
-            dma((6, n)),
+            dma((6,)),
             dma((6, outer)),
-            dma((6, outer)),
-            dma((2, outer, inner)),
-            dma((2, outer, inner)),
-            dma((2, outer, outer)),
-            dma((2, outer, outer)),
+            dma((1,)),
+            dma((4 + 2 * outer,)),
+            dma((1,)),
+            dma((outer,)),
+            dma((2,)),
             dma((2, outer)),
+            dma((2,)),
             dma((2, outer)),
+            dma((2,)),
+            dma((2,)),
+            dma((2,)),
+            dma((2,)),
+            dma((inner,)),
+            dma((inner,)),
         ],
         compiler_params=pltpu.CompilerParams(
             has_side_effects=True, collective_id=0, vmem_limit_bytes=40 * 1024 * 1024

time: 142 us -> 124 us (0.87)
  Pallas kernels: 141 us -> 123 us
    pallas_call x1, Pallas kernels: 138 us -> 120 us  [fused_shards(): pl.pallas_call(functools.partial(step_kernel, n, inner), out_shape=(pltpu...]
where the time goes in v2:
time: 124 us
  Pallas kernels  123 us (99%)
    pallas_call x1, Pallas kernels, fused_shards(): pl.pallas_call(functools.partial(step_kernel, n, inner), out_shape=(pltpu...  120 us
    pallas_call x1, Pallas kernels, fused_shards(): pl.pallas_call(hand_on, out_shape=(jax.ShapeDtypeStruct((keep, depth), bf...  3.48 us

profile of v2, /device:TPU:0, one launch (start us, length us, event | category | flops | bytes accessed | tf_op | source)
XLA Modules:
  0.0 123.6 jit_solution(10319336043703128061)
XLA Ops:
  0.6 119.5 %shard_map.144 = (bf16[16,2048]{1,0:T(8,128)(2,1)S(1)}, bf16[2,176,2048]{2,1,0:T(8,128)(2,1)S(1)}, bf16[2,176,2048]{2,1,0:T(8,128)(2,1)S(1)}, bf16[2,176,2048]{2...) custom-call(bf16[2,8,16,2048]{3,2,1,0:T(8,128)(2,1)} %bitcast.4, ...), custom_call_target="tpu_custom_call" | custom-call | tf_op jit(solution)/shard_map/pallas_call | solution.py:582
  120.2 3.5 %shard_map.145 = (bf16[16,2048]{1,0:T(8,128)(2,1)}, bf16[2,176,2048]{2,1,0:T(8,128)(2,1)}, bf16[2,176,2048]{2,1,0:T(8,128)(2,1)}, bf16[2,176,2048]{2,1,0:T(8,128...) custom-call(bf16[16,2048]{1,0:T(8,128)(2,1)S(1)} %get-tuple-element.21.refs_0_, ...), custom_call_target="tpu_custom_call" | custom-call | tf_op jit(solution)/shard_map/pallas_call | solution.py:641

commit v3 on v2

--- a/solution.py
+++ b/solution.py
@@ -138,6 +138,7 @@
     spread_recv,
     last_recv,
     last_pass,
+    ready,
 ):
     outer = n // inner
     me = lax.axis_index("fs")
@@ -406,48 +407,71 @@
         copy.start()
     load(0).start()
     barrier = pltpu.get_barrier_semaphore()
-    loop(
-        1,
-        n,
-        lambda j: pl.semaphore_signal(
-            barrier, inc=1, device_id={"fs": lax.rem(me + j, n)},
-            device_id_type=pl.DeviceIdType.MESH,
-        ),
-    )
-    pl.semaphore_signal(
-        barrier, inc=1, device_id={"tp": 1 - core}, device_id_type=pl.DeviceIdType.MESH
-    )
+    at_end = pl.when(ends)
+    at_mid = pl.when(jnp.logical_not(ends))
+
+    def signal(sem, **to):
+        pl.semaphore_signal(
+            sem, inc=1, device_id=to, device_id_type=pl.DeviceIdType.MESH
+        )
+
+    def opposite(sem):
+        for i in range(inner):
+            signal(sem, fs=planes[2] * inner + lax.rem(col + i, inner))
+
+    signal(barrier, fs=planes[1] * inner + col)
+    at_mid(lambda: opposite(barrier))
+    signal(barrier, tp=1 - core)
     for a in range(1, 6):
         load(a).start()
     side_loads[2].start()
     for copy in side_loads[:2]:
         copy.wait()
-    at_end = pl.when(ends)
-    at_mid = pl.when(jnp.logical_not(ends))
     cast(0)
-    pl.semaphore_wait(barrier, n)
-    at_mid(lambda: send(0, 2, 3, 1, 0))
-    at_end(lambda: send(0, 1, 0))
-    for a in (1, 2):
-        cast(a)
-        at_mid(lambda a=a: send(a, 2, 3, 1, 0))
-        at_end(lambda a=a: send(a, 1, 0))
+
+    @at_mid
+    def _():
+        pl.semaphore_wait(barrier, inner + 2)
+        opposite(ready.at[0])
+        send(0, 2)
+        cast(1)
+        send(1, 2)
+        pl.semaphore_wait(ready.at[0], inner)
+        for k in range(1, inner):
+            signal(ready.at[1], fs=row * inner + lax.rem(col + k, inner))
+        pl.semaphore_wait(ready.at[1], inner - 1)
+        signal(ready.at[2], fs=planes[1] * inner + col)
+        send(0, 3, 1, 0)
+        send(1, 3, 1, 0)
+        cast(2)
+        send(2, 2, 3, 1, 0)
+
+    @at_end
+    def _():
+        cast(1)
+        cast(2)
+        pl.semaphore_wait(barrier, 2)
+        pl.semaphore_wait(ready.at[2], 1)
+        for a in (0, 1, 2):
+            send(a, 1, 0)
+
     for a in (3, 4, 5):
         cast(a)
 
     @at_mid
     def _():
-        for a in (3, 4):
-            send(a, 2, 1, 0)
+        send(3, 2, 1, 0)
+        send(4, 1, 0)
         send(3, 3)
+        send(5, 1)
 
     @at_end
     def _():
         for a in (0, 1):
             send(a, 2, 3)
-        for a in (3, 4):
-            send(a, 1, 0)
+        send(3, 1, 0)
         send(2, 2, 3)
+        send(4, 1, 0)
 
     side_loads[2].wait()
     normalize_rows(lambda q: tokens_ref[:, q])
@@ -470,6 +494,7 @@
     arrive(2, far_mid)
     contract(2, 0, far_mid)
     start_plane(0, far_mid)
+    at_end(lambda: send(3, 3))
     hand_plane(0, far_end)
     for b in near:
         hand_twin(0, b)
@@ -478,7 +503,9 @@
     for b in (far_end, far_mid):
         hand_twin(0, b)
         cross_copy(0, b).start()
-    at_mid(lambda: send(4, 3))
+    at_mid(lambda: send(4, 2))
+    at_end(lambda: send(5, 1))
+    send(5, 0)
     for a in (3, 4):
         arrive_near(a)
     receive_cross(0)
@@ -487,43 +514,50 @@
     middle[spot] = own.astype(jnp.bfloat16)
     spread_line().start()
     spread_plane(spot)
-    send(5, 1, 0)
-    at_mid(lambda: send_last(3, 2))
+
+    @at_mid
+    def _():
+        send(4, 3)
+        send_last(3, 2)
 
     @at_end
     def _():
-        for g in (3, 2):
-            send(3, g)
-            send(4, g)
+        send(4, 3)
 
     spread_line().wait_recv()
     spread_plane(twin)
+
+    @at_end
+    def _():
+        send(3, 2)
+        send(4, 2)
+
     for a in (3, 4):
         arrive(a, far_end)
         arrive(a, far_mid)
     at_end(lambda: send(5, 2, 3))
-    arrive_near(5)
     counted(around, spread_send.at[1], spread_recv.at[1]).wait_recv()
     normalize_rows(lambda q: middle[q])
     for a in (3, 4):
         complete(a)
+    arrive_near(5)
     expand(3, 4)
     for b in near:
         contract(5, 1, b)
         start_plane(1, b)
+    at_mid(lambda: [hand_plane(1, b) for b in near] and None)
     arrive(5, far_end)
     contract(5, 1, far_end)
     start_part(columns(far_end), far_end)
-    for b in near:
-        hand_plane(1, b)
     arrive_last(0)
     for i in range(1, inner):
         arrive_last(i)
         contract_last(i - 1)
+    contract_last(inner - 1)
+    at_end(lambda: [hand_plane(1, b) for b in near] and None)
     for b in near:
         hand_twin(1, b)
         cross_copy(1, b).start()
-    contract_last(inner - 1)
     hand_part(far_end)
     hand_part(far_mid)
     for a in range(6):
@@ -549,12 +583,15 @@
 
 
 def hand_on(*refs):
-    sems = refs[-1]
+    sem = refs[-1].at[0]
     half = len(refs) // 2
-    copies = [
-        pltpu.make_async_copy(source, target, sems.at[i])
-        for i, (source, target) in enumerate(zip(refs[:half], refs[half : 2 * half]))
-    ]
+    copies = []
+    for source, target in zip(refs[:half], refs[half : 2 * half]):
+        rows = source.shape[-2] // 2
+        for part in range(2):
+            for lead in [()] if len(source.shape) == 2 else [(t,) for t in range(source.shape[0])]:
+                at = (*lead, pl.ds(part * rows, rows))
+                copies.append(pltpu.make_async_copy(source.at[at], target.at[at], sem))
     for copy in copies:
         copy.start()
     for copy in copies:
@@ -618,6 +655,7 @@
             dma((2,)),
             dma((inner,)),
             dma((inner,)),
+            pltpu.SemaphoreType.REGULAR((3,)),
         ],
         compiler_params=pltpu.CompilerParams(
             has_side_effects=True, collective_id=0, vmem_limit_bytes=40 * 1024 * 1024
@@ -644,7 +682,7 @@
         + (jax.ShapeDtypeStruct(served_shape, bf16),) * 6,
         in_specs=[anywhere] * 7,
         out_specs=(anywhere,) * 7,
-        scratch_shapes=[dma((7,))],
+        scratch_shapes=[dma((1,))],
         compiler_params=pltpu.CompilerParams(vmem_limit_bytes=1024 * 1024),
     )(*results)
     return (outs[0][None],) + tuple(outs[1:])

time: 124 us -> 120 us (0.968)
  Pallas kernels: 123 us -> 119 us
    pallas_call x1, Pallas kernels: 120 us -> 115 us  [fused_shards(): pl.pallas_call(functools.partial(step_kernel, n, inner), out_shape=(pltpu...]
where the time goes in v3:
time: 120 us; the launch traced here: 119 us
  Pallas kernels  119 us (99%)
    pallas_call x1, Pallas kernels, fused_shards(): pl.pallas_call(functools.partial(step_kernel, n, inner), out_shape=(pltpu...  115 us
    pallas_call x1, Pallas kernels, fused_shards(): pl.pallas_call(hand_on, out_shape=(jax.ShapeDtypeStruct((keep, depth), bf...  3.38 us

profile of v3, /device:TPU:0, one launch (start us, length us, event | category | flops | bytes accessed | tf_op | source)
XLA Modules:
  0.0 119.4 jit_solution(11701786819815436008)
XLA Ops:
  0.6 115.4 %shard_map.144 = (bf16[16,2048]{1,0:T(8,128)(2,1)S(1)}, bf16[2,176,2048]{2,1,0:T(8,128)(2,1)S(1)}, bf16[2,176,2048]{2,1,0:T(8,128)(2,1)S(1)}, bf16[2,176,2048]{2...) custom-call(bf16[2,8,16,2048]{3,2,1,0:T(8,128)(2,1)} %bitcast.4, ...), custom_call_target="tpu_custom_call" | custom-call | tf_op jit(solution)/shard_map/pallas_call | solution.py:619
  116.0 3.4 %shard_map.145 = (bf16[16,2048]{1,0:T(8,128)(2,1)}, bf16[2,176,2048]{2,1,0:T(8,128)(2,1)}, bf16[2,176,2048]{2,1,0:T(8,128)(2,1)}, bf16[2,176,2048]{2,1,0:T(8,128...) custom-call(bf16[16,2048]{1,0:T(8,128)(2,1)S(1)} %get-tuple-element.21.refs_0_, ...), custom_call_target="tpu_custom_call" | custom-call | tf_op jit(solution)/shard_map/pallas_call | solution.py:679

commit v4 on v3

--- a/solution.py
+++ b/solution.py
@@ -139,6 +139,8 @@
     last_recv,
     last_pass,
     ready,
+    stage_recv,
+    stage,
 ):
     outer = n // inner
     me = lax.axis_index("fs")
@@ -188,13 +190,13 @@
         own = pl.ds(pl.multiple_of(me * rows, rows), rows)
         served[a][core, :, mine] = cut[a, own, :]
 
-    def block_copy(a, g, i, recvs=None):
+    def block_copy(a, g, i):
         to = planes[g] * inner + lax.rem(col + i, inner)
         return pltpu.make_async_remote_copy(
             src_ref=cut.at[a, pl.ds(pl.multiple_of(to * rows, rows), rows), :],
             dst_ref=served[a].at[core, :, mine],
             send_sem=send_sem.at[a],
-            recv_sem=recv_sem.at[a, row] if recvs is None else recvs.at[i],
+            recv_sem=recv_sem.at[a, row],
             device_id={"fs": to},
             device_id_type=pl.DeviceIdType.MESH,
         )
@@ -203,9 +205,55 @@
         for g in groups:
             loop(1 if g == 0 else 0, inner, lambda i, g=g: block_copy(a, g, i).start())
 
-    def send_last(*groups):
-        for g in groups:
-            loop(0, inner, lambda i, g=g: block_copy(5, g, i, last_recv).start())
+    def unit_rows(to):
+        return pl.ds(pl.multiple_of(to * rows, rows), rows)
+
+    def feature_cols(at):
+        return pl.ds(pl.multiple_of(at * feats, feats), feats)
+
+    staged = (4, 5)
+
+    def stage_own(a):
+        for f in (0, 1):
+            to = planes[2 + f] * inner + col
+            stage[staged.index(a), f, :, feature_cols(col)] = cut[a, unit_rows(to), :]
+
+    def stage_out(a):
+        for f in (0, 1):
+            for k in range(1, inner):
+                there = lax.rem(col + k, inner)
+                pltpu.make_async_remote_copy(
+                    src_ref=cut.at[a, unit_rows(planes[2 + f] * inner + there), :],
+                    dst_ref=stage.at[staged.index(a), f, :, feature_cols(col)],
+                    send_sem=send_sem.at[a],
+                    recv_sem=stage_recv.at[staged.index(a)],
+                    device_id={"fs": row * inner + there},
+                    device_id_type=pl.DeviceIdType.MESH,
+                ).start()
+
+    def stage_wait(a):
+        ref = stage.at[staged.index(a), :, :, pl.ds(0, (inner - 1) * feats)]
+        counted(ref, send_sem.at[a], stage_recv.at[staged.index(a)]).wait_recv()
+
+    def stage_copy(a, f, at, into, recvs):
+        return pltpu.make_async_remote_copy(
+            src_ref=stage.at[staged.index(a), f, :, at],
+            dst_ref=served[a].at[core, :, into],
+            send_sem=send_sem.at[a],
+            recv_sem=recvs,
+            device_id={"fs": planes[2 + f] * inner + col},
+            device_id_type=pl.DeviceIdType.MESH,
+        )
+
+    def send_last(*fs):
+        for f in fs:
+            for i in range(inner):
+                at = pl.ds(i * feats, feats)
+                stage_copy(5, f, at, feature_cols(row * inner + i), last_recv.at[i]).start()
+
+    def send_whole(a, *fs):
+        for f in fs:
+            stage_copy(a, f, slice(None), columns(row), recv_sem.at[a, row]).start()
 
     def counted(ref, sends, recvs):
         return pltpu.make_async_remote_copy(
@@ -370,8 +418,7 @@
         product(d, block, columns(b))
 
     def last_at(i):
-        source = far_mid * inner + lax.rem(col + inner - i, inner)
-        return pl.ds(pl.multiple_of(source * feats, feats), feats)
+        return feature_cols(far_mid * inner + i)
 
     def last_copy(i):
         return counted(
@@ -461,7 +508,7 @@
     @at_mid
     def _():
         send(3, 2, 1, 0)
-        send(4, 1, 0)
+        send(4, 1)
         send(3, 3)
         send(5, 1)
 
@@ -471,8 +518,11 @@
             send(a, 2, 3)
         send(3, 1, 0)
         send(2, 2, 3)
-        send(4, 1, 0)
-
+        send(4, 1)
+
+    for a in staged:
+        stage_own(a)
+        stage_out(a)
     side_loads[2].wait()
     normalize_rows(lambda q: tokens_ref[:, q])
     for a in (0, 1, 2):
@@ -503,11 +553,11 @@
     for b in (far_end, far_mid):
         hand_twin(0, b)
         cross_copy(0, b).start()
-    at_mid(lambda: send(4, 2))
+    stage_wait(4)
+    at_mid(lambda: send_whole(4, 0))
     at_end(lambda: send(5, 1))
+    send(4, 0)
     send(5, 0)
-    for a in (3, 4):
-        arrive_near(a)
     receive_cross(0)
     branch = summed[0].astype(jnp.float32) + across[0].astype(jnp.float32)
     own = tokens_ref[:, spot].astype(jnp.float32) + 0.5 * branch
@@ -515,27 +565,23 @@
     spread_line().start()
     spread_plane(spot)
 
-    @at_mid
-    def _():
-        send(4, 3)
-        send_last(3, 2)
-
-    @at_end
-    def _():
-        send(4, 3)
+    send_whole(4, 1)
 
     spread_line().wait_recv()
     spread_plane(twin)
+    stage_wait(5)
+    at_mid(lambda: send_last(1, 0))
 
     @at_end
     def _():
         send(3, 2)
-        send(4, 2)
+        send_whole(4, 0)
 
     for a in (3, 4):
+        arrive_near(a)
         arrive(a, far_end)
         arrive(a, far_mid)
-    at_end(lambda: send(5, 2, 3))
+    at_end(lambda: send_whole(5, 0, 1))
     counted(around, spread_send.at[1], spread_recv.at[1]).wait_recv()
     normalize_rows(lambda q: middle[q])
     for a in (3, 4):
@@ -555,15 +601,18 @@
         contract_last(i - 1)
     contract_last(inner - 1)
     at_end(lambda: [hand_plane(1, b) for b in near] and None)
+    hand_part(far_end)
     for b in near:
         hand_twin(1, b)
         cross_copy(1, b).start()
-    hand_part(far_end)
     hand_part(far_mid)
     for a in range(6):
         spent = cut.at[a, pl.ds(0, (n - 1) * rows), :]
         counted(spent, send_sem.at[a], recv_sem.at[a, 0]).wait_send()
         counted(served[a].at[core], pass_send.at[0], pass_recv.at[0]).wait_send()
+    for a in staged:
+        spent = cut.at[a, pl.ds(0, 2 * (inner - 1) * rows), :]
+        counted(spent, send_sem.at[a], recv_sem.at[a, 0]).wait_send()
     spread_line().wait_send()
     counted(around, spread_send.at[1], spread_recv.at[1]).wait_send()
     two = pl.ds(0, 2 * band)
@@ -656,6 +705,8 @@
             dma((inner,)),
             dma((inner,)),
             pltpu.SemaphoreType.REGULAR((3,)),
+            dma((2,)),
+            pltpu.VMEM((2, 2, rows, depth // outer), bf16),
         ],
         compiler_params=pltpu.CompilerParams(
             has_side_effects=True, collective_id=0, vmem_limit_bytes=40 * 1024 * 1024

time: 120 us -> 118 us (0.983)
  Pallas kernels: 119 us -> 117 us
    pallas_call x1, Pallas kernels: 115 us -> 114 us  [fused_shards(): pl.pallas_call(functools.partial(step_kernel, n, inner), out_shape=(pltpu...]
where the time goes in v4:
time: 118 us
  Pallas kernels  117 us (99%)
    pallas_call x1, Pallas kernels, fused_shards(): pl.pallas_call(functools.partial(step_kernel, n, inner), out_shape=(pltpu...  114 us
    pallas_call x1, Pallas kernels, fused_shards(): pl.pallas_call(hand_on, out_shape=(jax.ShapeDtypeStruct((keep, depth), bf...  3.38 us

profile of v4, /device:TPU:0, one launch (start us, length us, event | category | flops | bytes accessed | tf_op | source)
XLA Modules:
  0.0 117.8 jit_solution(15305664132468162531)
XLA Ops:
  0.6 113.8 %shard_map.144 = (bf16[16,2048]{1,0:T(8,128)(2,1)S(1)}, bf16[2,176,2048]{2,1,0:T(8,128)(2,1)S(1)}, bf16[2,176,2048]{2,1,0:T(8,128)(2,1)S(1)}, bf16[2,176,2048]{2...) custom-call(bf16[2,8,16,2048]{3,2,1,0:T(8,128)(2,1)} %bitcast.4, ...), custom_call_target="tpu_custom_call" | custom-call | tf_op jit(solution)/shard_map/pallas_call | solution.py:668
  114.4 3.4 %shard_map.145 = (bf16[16,2048]{1,0:T(8,128)(2,1)}, bf16[2,176,2048]{2,1,0:T(8,128)(2,1)}, bf16[2,176,2048]{2,1,0:T(8,128)(2,1)}, bf16[2,176,2048]{2,1,0:T(8,128...) custom-call(bf16[16,2048]{1,0:T(8,128)(2,1)S(1)} %get-tuple-element.21.refs_0_, ...), custom_call_target="tpu_custom_call" | custom-call | tf_op jit(solution)/shard_map/pallas_call | solution.py:730

commit v5 on v4

--- a/solution.py
+++ b/solution.py
@@ -499,7 +499,7 @@
         cast(2)
         pl.semaphore_wait(barrier, 2)
         pl.semaphore_wait(ready.at[2], 1)
-        for a in (0, 1, 2):
+        for a in (0, 1):
             send(a, 1, 0)
 
     for a in (3, 4, 5):
@@ -516,6 +516,7 @@
     def _():
         for a in (0, 1):
             send(a, 2, 3)
+        send(2, 1, 0)
         send(3, 1, 0)
         send(2, 2, 3)
         send(4, 1)
@@ -577,13 +578,15 @@
         send(3, 2)
         send_whole(4, 0)
 
-    for a in (3, 4):
-        arrive_near(a)
-        arrive(a, far_end)
-        arrive(a, far_mid)
-    at_end(lambda: send_whole(5, 0, 1))
+    arrive_near(3)
+    arrive_near(4)
+    arrive(3, far_end)
+    arrive(3, far_mid)
+    arrive(4, far_end)
     counted(around, spread_send.at[1], spread_recv.at[1]).wait_recv()
     normalize_rows(lambda q: middle[q])
+    arrive(4, far_mid)
+    at_end(lambda: send_whole(5, 0, 1))
     for a in (3, 4):
         complete(a)
     arrive_near(5)

time: 118 us -> 118 us (level)
  no operation moved by 1% of the time
where the time goes in v5:
time: 118 us
  Pallas kernels  117 us (99%)
    pallas_call x1, Pallas kernels, fused_shards(): pl.pallas_call(functools.partial(step_kernel, n, inner), out_shape=(pltpu...  114 us
    pallas_call x1, Pallas kernels, fused_shards(): pl.pallas_call(hand_on, out_shape=(jax.ShapeDtypeStruct((keep, depth), bf...  3.38 us

profile of v5, /device:TPU:0, one launch (start us, length us, event | category | flops | bytes accessed | tf_op | source)
XLA Modules:
  0.0 117.6 jit_solution(16239979670695344630)
XLA Ops:
  0.6 113.6 %shard_map.144 = (bf16[16,2048]{1,0:T(8,128)(2,1)S(1)}, bf16[2,176,2048]{2,1,0:T(8,128)(2,1)S(1)}, bf16[2,176,2048]{2,1,0:T(8,128)(2,1)S(1)}, bf16[2,176,2048]{2...) custom-call(bf16[2,8,16,2048]{3,2,1,0:T(8,128)(2,1)} %bitcast.4, ...), custom_call_target="tpu_custom_call" | custom-call | tf_op jit(solution)/shard_map/pallas_call | solution.py:671
  114.3 3.4 %shard_map.145 = (bf16[16,2048]{1,0:T(8,128)(2,1)}, bf16[2,176,2048]{2,1,0:T(8,128)(2,1)}, bf16[2,176,2048]{2,1,0:T(8,128)(2,1)}, bf16[2,176,2048]{2,1,0:T(8,128...) custom-call(bf16[16,2048]{1,0:T(8,128)(2,1)S(1)} %get-tuple-element.21.refs_0_, ...), custom_call_target="tpu_custom_call" | custom-call | tf_op jit(solution)/shard_map/pallas_call | solution.py:733
